TPU v7x, 128 devices: a whole 4x4x4 slice. The times are simulated.
128 devices in a mesh: ep: 32 (over z, y, core), tp: 4 (over x).
Axes of the slice: x: 4, y: 4, z: 4, core: 2. Of those that a mesh axis runs over, the one named last changes fastest.
Arguments:
- queries: bfloat16 [32768, 1024], P('ep', 'tp'), may hold values from -6 to 6
- keys: bfloat16 [32768, 1024], P('ep', 'tp'), may hold values from -6 to 6
- values: bfloat16 [32768, 2048], P('ep', 'tp'), may hold values from -6 to 6
- log_input_gate: float32 [32768, 8], P('ep', 'tp'), may hold values from -6 to 103
- forget_preactivation: float32 [32768, 8], P('ep', 'tp'), may hold values from 0 to 16
- forget_offset: float32 [32768, 8], P('ep', 'tp'), may hold values from -0.7 to 0
- head_norm_scale: float32 [2048], P('tp'), may hold values from 0.1 to 1.9
- memory_output_weight: bfloat16 [2048, 4096], P('tp'), may hold values from -0.125 to 0.125
- second_micro_tokens: bfloat16 [16384, 4096], P('ep'), may hold values from -6 to 6
- expert_norm_scale: float32 [4096], replicated, may hold values from 0.1 to 1.9
- expert_choice_index: int32 [16384, 2], P('ep'), may hold values from 0 to 63, all different within a row; in each aligned block of 512 rows (0 to 511, 512 to 1023, ...) at most 24 rows name the same one
- group_likelihood: float32 [16384], P('ep'), may hold values from 0.2 to 1
- expert_raw_weight: float32 [16384, 2], P('ep'), may hold values from 0.1 to 1
- gate_weight: bfloat16 [64, 4096, 1024], P('ep', None, 'tp'), may hold values from -0.09375 to 0.09375
- up_weight: bfloat16 [64, 4096, 1024], P('ep', None, 'tp'), may hold values from -0.09375 to 0.09375
- down_weight: bfloat16 [64, 1024, 4096], P('ep', 'tp'), may hold values from -0.1875 to 0.1875
Outputs:
- mixed: bfloat16 [32768, 4096], P(('ep', 'tp'))
- routed: bfloat16 [16384, 4096], P('ep', 'tp')
Inputs may be any that keep to these rules, and one draw needn't show every extreme that they name: `expert_choice_index`: each row names 2 different experts. Within the 512 rows of one index of ep (aligned blocks) no expert is named more than 24 times, and in some blocks one expert is named exactly 24 times.
All inputs are finite; a program needn't handle non-finite values.
Results may differ from a plain program's by a relative error of at most 0.012.
Values may be sent and summed in bfloat16 or wider, within the bound.
No kernel may reach another device: no remote copies, remote signals or barrier semaphores. Data moves between devices by JAX's collectives and lax.ppermute only.
A program may use at most 192 MiB of HBM per device.

v0:
```python
import math
import jax
import jax.numpy as jnp
from jax import lax
from jax.sharding import Mesh
from jax.sharding import PartitionSpec as P

BLOCK = 128
EP = ("ep_0", "ep_1", "ep_2")
EP_TP = ("ep_0", "ep_1", "ep_2", "tp")
EPSILON = 1e-06
FLOOR_LOG = -1e30


def filled_with(value, identity):
    return jax.tree.map(
        lambda a, e: jnp.broadcast_to(jnp.asarray(e, a.dtype), a.shape), value, identity
    )


def collected_together(value, axis):
    leaves = jax.tree.leaves(value)
    order = sorted(range(len(leaves)), key=lambda k: -leaves[k].size)
    width = (1, *leaves[order[0]].shape)[-1]
    lines = [
        jnp.pad(leaves[k].reshape(-1), (0, -leaves[k].size % width)).reshape(-1, width)
        for k in order
    ]
    both, at, found = (lax.all_gather(jnp.concatenate(lines), axis), 0, {})
    for k, line in zip(order, lines):
        share = both[:, at : at + len(line)].reshape(len(both), -1)
        found[k] = share[:, : leaves[k].size].reshape(-1, *leaves[k].shape)
        at += len(line)
    numbers = iter(range(len(leaves)))
    return jax.tree.map(lambda _: found[next(numbers)], value)


def entering(value, axes, combine, identity):
    before = start = filled_with(value, identity)
    subtotal = value
    for axis in reversed(axes):
        peers, position = (lax.axis_size(axis), lax.axis_index(axis))
        pieces = collected_together(subtotal, axis)
        inside, subtotal = (start, start)
        for k in range(peers):
            passed = k < position
            subtotal = combine(subtotal, jax.tree.map(lambda part: part[k], pieces))
            inside = jax.tree.map(lambda new, old: jnp.where(passed, new, old), subtotal, inside)
        before = combine(inside, before)
    return before


def merge_states(earlier, later):
    memory_one, stable_one, total_one = earlier
    memory_two, stable_two, total_two = later
    highest = jnp.maximum(total_two + stable_one, stable_two)
    weight_one = jnp.exp(total_two + stable_one - highest)
    weight_two = jnp.exp(stable_two - highest)
    memory = weight_one[..., None, None] * memory_one + weight_two[..., None, None] * memory_two
    return (memory, highest, total_one + total_two)


def advance(carry, piece):
    return (merge_states(carry, piece), carry)


def recurrence_portion(
    queries,
    keys,
    values,
    log_input_gate,
    forget_preactivation,
    forget_offset,
    head_norm_scale,
    memory_output_weight,
):
    row_count, head_count = log_input_gate.shape
    key_width = queries.shape[1] // head_count
    value_width = values.shape[1] // head_count
    block_count = row_count // BLOCK
    qk_scale = 1.0 / math.sqrt(key_width)
    query_blocks = queries.reshape(block_count, BLOCK, head_count, key_width)
    key_blocks = keys.reshape(block_count, BLOCK, head_count, key_width)
    value_blocks = values.reshape(block_count, BLOCK, head_count, value_width)
    key_float = key_blocks.astype(jnp.float32) * qk_scale
    forget_log_factor = jax.nn.log_sigmoid(forget_preactivation) + forget_offset
    forget_log_factor = forget_log_factor.reshape(block_count, BLOCK, head_count).transpose(0, 2, 1)
    in_gate = log_input_gate.reshape(block_count, BLOCK, head_count).transpose(0, 2, 1)
    running = jnp.cumsum(forget_log_factor, axis=-1)
    totals = running[..., -1]
    to_end = totals[..., None] - running + in_gate
    block_peak = jnp.max(to_end, axis=-1)
    key_weight = jnp.exp(to_end - block_peak[..., None])
    weighted_keys = (key_float * key_weight.transpose(0, 2, 1)[..., None]).astype(jnp.bfloat16)
    block_memory = jnp.einsum(
        "bshd,bshe->bhde", weighted_keys, value_blocks, preferred_element_type=jnp.float32
    )
    empty = (
        jnp.zeros((head_count, key_width, value_width), jnp.float32),
        jnp.full((head_count,), FLOOR_LOG, jnp.float32),
        jnp.zeros((head_count,), jnp.float32),
    )
    device_state, starts = lax.scan(advance, empty, (block_memory, block_peak, totals))
    incoming = entering(device_state, EP, merge_states, empty)
    memory, peak, unused = merge_states(incoming, starts)
    scores = (
        jnp.einsum("bthd,bshd->bhts", query_blocks, key_blocks, preferred_element_type=jnp.float32)
        * qk_scale
    )
    causal = jnp.tril(jnp.ones((BLOCK, BLOCK), dtype=bool))
    log_weight = running[..., :, None] - running[..., None, :] + in_gate[..., None, :]
    log_weight = jnp.where(causal, log_weight, -jnp.inf)
    carried = running + peak[..., None]
    stable = jnp.maximum(carried, jnp.max(log_weight, axis=-1))
    inner = (scores * jnp.exp(log_weight - stable[..., None])).astype(jnp.bfloat16)
    outer = jnp.exp(carried - stable)
    memory_half = memory.astype(jnp.bfloat16)
    state = outer[..., None] * jnp.einsum(
        "bthd,bhde->bhte", query_blocks, memory_half, preferred_element_type=jnp.float32
    )
    state = state + jnp.einsum(
        "bhts,bshe->bhte", inner, value_blocks, preferred_element_type=jnp.float32
    )
    state = state * lax.rsqrt(jnp.mean(state * state, axis=-1, keepdims=True) + EPSILON)
    hidden = state.transpose(0, 2, 1, 3).reshape(row_count, head_count * value_width)
    hidden = (hidden * head_norm_scale).astype(jnp.bfloat16)
    return lax.psum_scatter(
        jnp.dot(hidden, memory_output_weight, preferred_element_type=jnp.float32).astype(
            jnp.bfloat16
        ),
        "tp",
        scatter_dimension=0,
        tiled=True,
    )


def expert_half(
    second_micro_tokens,
    expert_norm_scale,
    expert_choice_index,
    group_likelihood,
    expert_raw_weight,
    gate_weight,
    up_weight,
    down_weight,
):
    token_count, model_width = second_micro_tokens.shape
    pick_count = expert_choice_index.shape[1]
    local_experts = gate_weight.shape[0]
    ep_size = lax.axis_size(EP)
    tp_size = lax.axis_size("tp")
    expert_count = local_experts * ep_size
    capacity = tp_size * max(1, 3 * pick_count * token_count // (2 * expert_count * tp_size))
    token_float = second_micro_tokens.astype(jnp.float32)
    normed = token_float * lax.rsqrt(
        jnp.mean(token_float * token_float, axis=-1, keepdims=True) + EPSILON
    )
    normed = (normed * expert_norm_scale).astype(jnp.bfloat16)
    share = expert_raw_weight / jnp.sum(expert_raw_weight, axis=1, keepdims=True)
    route_weight = group_likelihood[:, None] * share
    flat_expert = expert_choice_index.reshape(-1)
    one_hot = (flat_expert[:, None] == jnp.arange(expert_count, dtype=jnp.int32)[None, :]).astype(
        jnp.int32
    )
    slot_rank = jnp.sum(jnp.cumsum(one_hot, axis=0) * one_hot, axis=1) - 1
    owner = flat_expert // local_experts
    local_index = flat_expert % local_experts
    slot_index = owner * (local_experts * capacity) + local_index * capacity + slot_rank
    slot_total = local_experts * ep_size * capacity
    token_index = jnp.arange(token_count * pick_count, dtype=jnp.int32) // pick_count
    slot_token = jnp.zeros((slot_total,), jnp.int32).at[slot_index].set(token_index)
    slot_used = jnp.zeros((slot_total,), bool).at[slot_index].set(True)
    outgoing = jnp.where(slot_used[:, None], normed[slot_token], jnp.zeros((), jnp.bfloat16))
    outgoing = outgoing.reshape(ep_size, local_experts, capacity, model_width)
    arrived = lax.all_to_all(outgoing, EP, split_axis=0, concat_axis=0, tiled=True)
    gate = jnp.einsum("serd,edf->serf", arrived, gate_weight, preferred_element_type=jnp.float32)
    upward = jnp.einsum("serd,edf->serf", arrived, up_weight, preferred_element_type=jnp.float32)
    hidden = (jax.nn.silu(gate) * upward).astype(jnp.bfloat16)
    unit_width = down_weight.shape[1]
    own_columns = lax.all_to_all(down_weight, "tp", split_axis=2, concat_axis=1, tiled=True)
    column_count = own_columns.shape[2]
    zero_total = jnp.zeros((column_count, ep_size, local_experts, capacity), jnp.float32)
    total = zero_total
    piece = lax.all_gather(hidden, "tp", axis=3, tiled=True)
    for group in range(piece.shape[3] // unit_width):
        group_units = piece[:, :, :, group * unit_width : (group + 1) * unit_width]
        down_rows = lax.dynamic_slice_in_dim(own_columns, group * unit_width, unit_width, 1)
        partial_value = jnp.einsum(
            "serf,efc->cser", group_units, down_rows, preferred_element_type=jnp.float32
        ).astype(jnp.bfloat16)
        total = total + lax.optimization_barrier(partial_value).astype(jnp.float32)
    finished = total.astype(jnp.bfloat16)
    returned = lax.all_to_all(finished, EP, split_axis=1, concat_axis=1, tiled=True)
    flat_result = returned.reshape(returned.shape[0], slot_total)
    picked = jnp.take(flat_result, slot_index, axis=1).astype(jnp.float32)
    picked = picked.reshape(flat_result.shape[0], token_count, pick_count)
    combined = jnp.sum(picked * route_weight[None], axis=2)
    return combined.T.astype(jnp.bfloat16)


def per_device(
    queries,
    keys,
    values,
    log_input_gate,
    forget_preactivation,
    forget_offset,
    head_norm_scale,
    memory_output_weight,
    second_micro_tokens,
    expert_norm_scale,
    expert_choice_index,
    group_likelihood,
    expert_raw_weight,
    gate_weight,
    up_weight,
    down_weight,
):
    mixed = recurrence_portion(
        queries,
        keys,
        values,
        log_input_gate,
        forget_preactivation,
        forget_offset,
        head_norm_scale,
        memory_output_weight,
    )
    routed = expert_half(
        second_micro_tokens,
        expert_norm_scale,
        expert_choice_index,
        group_likelihood,
        expert_raw_weight,
        gate_weight,
        up_weight,
        down_weight,
    )
    return (mixed, routed)


def solution(mesh):
    split = Mesh(mesh.devices.reshape(4, 4, 2, mesh.shape["tp"]), ("ep_0", "ep_1", "ep_2", "tp"))
    placed = (
        P(EP, "tp"),
        P(EP, "tp"),
        P(EP, "tp"),
        P(EP, "tp"),
        P(EP, "tp"),
        P(EP, "tp"),
        P("tp"),
        P("tp", None),
        P(EP, None),
        P(),
        P(EP, None),
        P(EP),
        P(EP, None),
        P(EP, None, "tp"),
        P(EP, None, "tp"),
        P(EP, "tp", None),
    )
    return jax.shard_map(
        per_device,
        mesh=split,
        in_specs=placed,
        out_specs=(P(EP_TP, None), P(EP, "tp")),
        check_vma=False,
    )
```

profile of v0, /device:TPU:2, one launch (start us, length us, event | category | flops | bytes accessed | tf_op | source)
XLA Modules:
  0.0 469.7 jit_solution(17323385805331098350)
XLA Ops:
  9.4 18.0 %reduce-window.6 = s32[64,8,128]{2,1,0:T(8,128)S(1)} reduce-window(s32[64,8,128]{2,1,0:T(8,128)S(1)} %fusion.71, s32[]{:T(128)} %constant.116.clone.1), window={size=1x1x128 pad=0_0x0_0x127_0}, to_apply=%region_7.8 | reduce-window | flops 8323072 | bytes 524292 | tf_op jit(solution)/shard_map/reduce-window
  28.1 4.3 scatter_custom_fusion.1
  32.4 3.1 fusion.12
  35.5 4.6 scatter_custom_fusion
  40.3 5.8 %fusion.14 = bf16[512,4096]{1,0:T(8,128)(2,1)} fusion(bf16[512,4096]{1,0:T(8,128)(2,1)} %param.26, f32[4096]{0:T(1024)S(1)} %copy-done.10, f32[512]{0:T(512)S(1)} %add_rsqrt_fusion), kind=kLoop, calls=%fused_computation.29 | loop fusion | flops 8388608 | bytes 8407040 | tf_op jit(solution)/shard_map/convert_element_type | solution.py:158
  46.1 24.8 %gather_fusion = bf16[1536,4096]{1,0:T(8,128)(2,1)} fusion(bf16[512,4096]{1,0:T(8,128)(2,1)} %fusion.14, s32[2048]{0:T(1024)S(1)} %pad_clamp_fusion), kind=kCustom, calls=%fused_computation | custom fusion | bytes 25171968 | tf_op jit(solution)/shard_map/gather | solution.py:173
  70.9 10.7 %broadcast_select_fusion.2 = bf16[32,2,24,4096]{3,2,1,0:T(8,128)(2,1)} fusion(bf16[32,2,24,4096]{3,2,1,0:T(8,128)(2,1)} %bitcast.456, pred[32,2,24]{2,1,0:T(4,128)(4,1)S(1)} %broadcast_in_dim.57), kind=kLoop, calls=%fused_computation.20 | loop fusion | flops 6291456 | bytes 25167360 | tf_op jit(solution)/shard_map/jit(_where)/select_n | solution.py:173
  81.6 8.6 %all-to-all-start = ((bf16[32,2,24,4096]{3,2,1,0:T(8,128)(2,1)}), bf16[32,2,24,4096]{3,2,1,0:T(8,128)(2,1)}, u32[]{:S(2)}, u32[]{:S(2)}) async-start(bf16[32,2,24,4096]{3,2,1,0:T(8,128)(2,1)} %broadcast_select_fusion.2), calls=%async_computation.1 | async-start | bytes 25165824 | tf_op jit(solution)/shard_map/all_to_all | solution.py:175
  94.4 7.8 %while.21 = (s32[]{:T(128)}, f32[2,128,256]{2,1,0:T(8,128)S(1)}, f32[2]{0:T(128)S(1)}, f32[2]{0:T(128)S(1)}, f32[8,2,128,256]{3,2,1,0:T(8,128)}, /*index=5*/f32[...) while((s32[]{:T(128)}, f32[2,128,256]{2,1,0:T(8,128)S(1)}, ...), condition=%wide.region_3.4_spmd.clone, body=%wide.region_2.3_spmd.clone.sunk | while | flops 327699 | bytes 1311534 | solution.py:103
  105.9 42.7 %all-gather.12.cloned.1.call-done = f32[4,258,256]{2,1,0:T(8,128)} async-done(((f32[1,258,256]{2,1,0:T(8,128)}), f32[4,258,256]{2,1,0:T(8,128)}) %all-gather.12.cloned.1.call-update) | async-done | bytes 1056784 | tf_op jit(solution)/shard_map/all_gather | solution.py:29
  157.4 79.3 %all-gather.14.cloned.1.call-done = f32[4,258,256]{2,1,0:T(8,128)} async-done(((f32[1,258,256]{2,1,0:T(8,128)}), f32[4,258,256]{2,1,0:T(8,128)}) %all-gather.14.cloned.1.call-update) | async-done | bytes 1056784 | tf_op jit(solution)/shard_map/all_gather | solution.py:29
  237.5 19.7 %all-to-all-done = bf16[32,2,24,4096]{3,2,1,0:T(8,128)(2,1)} async-done(((bf16[32,2,24,4096]{3,2,1,0:T(8,128)(2,1)}), bf16[32,2,24,4096]{3,2,1,0:T(8,128)(2,1)}, u32[]{:S(2)}, u32[]{:S(2)}) %all-to-all-start) | async-done | bytes 12582944 | tf_op jit(solution)/shard_map/all_to_all | solution.py:175
  257.2 7.6 %fusion.10 = f32[2,32,24,256]{3,2,1,0:T(8,128)S(1)} fusion(bf16[32,2,24,4096]{3,2,1,0:T(8,128)(2,1)} %all-to-all-done, bf16[2,4096,256]{2,1,0:T(8,128)(2,1)} %param.31), kind=kOutput, calls=%fused_computation.23 | convolution fusion | flops 3221225472 | bytes 18350080 | tf_op jit(solution)/shard_map/serd,edf->serf/dot_general | solution.py:176
  264.8 10.3 %fusion.21 = bf16[32,2,24,256]{3,2,0,1:T(8,128)(2,1)} fusion(f32[2,32,24,256]{3,2,1,0:T(8,128)S(1)} %fusion.10, bf16[2,4096,256]{2,1,0:T(8,128)(2,1)} %param.32, bf16[32,2,24,4096]{3,2,1,0:T(8,128)(2,1)} %all-to-all-done), kind=kOutput, calls=%fused_computation.50 | convolution fusion | flops 3223584768 | bytes 19136512 | tf_op jit(solution)/shard_map/serd,edf->serf/dot_general | solution.py:177
  280.0 3.7 fusion.19
  288.0 7.5 %convolution_convert_fusion = bf16[1024,4096]{1,0:T(8,128)(2,1)} fusion(bf16[512,4096]{1,0:T(8,128)(2,1)S(1)} %copy-done.16, f32[64,8,8,128]{3,2,1,0:T(8,128)S(1)} %bitcast.464, f32[512]{0:T(512)S(1)} %copy-done.17), kind=kOutput, calls=%fused_computation.30 | convolution fusion | flops 4300210176 | bytes 14682112 | tf_op jit(solution)/shard_map/dot_general | solution.py:128
  295.6 11.1 %copy.166 = bf16[2,256,4096]{1,0,2:T(2,128)(2,1)} copy(bf16[2,256,4096]{2,1,0:T(8,128)(2,1)} %param.33) | data formatting | bytes 8388608 | tf_op args[15]
  306.7 67.7 %all_to_all.28 = bf16[2,256,4096]{1,0,2:T(2,128)(2,1)} all-to-all(bf16[2,256,4096]{1,0,2:T(2,128)(2,1)} %copy.166), channel_id=1, replica_groups=mesh['ep_0'=4,'ep_1'=4,'ep_2'=2,'tp'=4] {'tp'}, dimensions={2} | all-to-all | bytes 8388608 | tf_op jit(solution)/shard_map/all_to_all | solution.py:180
  374.4 11.3 %copy.167 = bf16[2,256,4,1024]{3,1,2,0:T(8,128)(2,1)} copy(bf16[2,256,4,1024]{1,0,3,2:T(2,128)(2,1)} %bitcast.462) | data formatting | bytes 8388608 | tf_op jit(solution)/shard_map/all_to_all | solution.py:180
  393.0 3.2 add_convert_fusion
  398.3 4.2 all-to-all-start.2
  403.3 41.2 %all-to-all-done.2 = bf16[1024,32,2,24]{0,3,2,1:T(8,128)(2,1)S(1)} async-done(((bf16[1024,32,2,24]{0,3,2,1:T(8,128)(2,1)}), bf16[1024,32,2,24]{0,3,2,1:T(8,128)(2,1)S(1)}, u32[]{:S(2)}, u32[]{:S(2)}) %all-to-all-start.2) | async-done | bytes 3145760 | tf_op jit(solution)/shard_map/all_to_all | solution.py:193
  444.5 5.4 %gather_fusion.1 = bf16[1024,1024]{1,0:T(8,128)(2,1)} fusion(bf16[1024,1536]{0,1:T(8,128)(2,1)S(1)} %bitcast.455, s32[1024]{0:T(1024)S(1)} %broadcast_clamp_fusion), kind=kCustom, calls=%fused_computation.1 | custom fusion | bytes 4198400 | tf_op jit(solution)/shard_map/jit(_take)/gather | solution.py:195
  452.6 9.4 %multiply_reduce_fusion = bf16[1024,512]{0,1:T(8,128)(2,1)} fusion(bf16[1024,512,2]{0,2,1:T(2,128)(2,1)S(1)} %gather.14, pred[512,2]{1,0:T(8,128)(4,1)S(1)} %copy.162, f32[512,2]{1,0:T(8,128)S(1)} %copy.169), kind=kLoop, calls=%fused_computation.34 | loop fusion | flops 3670016 | bytes 3150848 | tf_op jit(solution)/shard_map/reduce_sum | solution.py:197
  (218 shorter events, 48.7 us)
Async XLA Ops:
  9.4 30.9 %copy-start.10 = (f32[4096]{0:T(1024)S(1)}, f32[4096]{0:T(1024)}, u32[]{:S(2)}) copy-start(f32[4096]{0:T(1024)} %param.27) | copy-start | bytes 49156
  81.5 8.7 %copy-start.13 = (f32[1024,2]{0,1:T(2,128)S(1)}, f32[1024,2]{0,1:T(2,128)}, u32[]{:S(2)}) copy-start(f32[1024,2]{0,1:T(2,128)} %param.23) | copy-start | bytes 24580
  81.5 8.7 %copy-start.14 = (f32[1024,2]{0,1:T(2,128)S(1)}, f32[1024,2]{0,1:T(2,128)}, u32[]{:S(2)}) copy-start(f32[1024,2]{0,1:T(2,128)} %param.22) | copy-start | bytes 24580
  81.5 9.5 %copy-start.9 = (f32[1024,2]{0,1:T(2,128)S(1)}, f32[1024,2]{0,1:T(2,128)}, u32[]{:S(2)}) copy-start(f32[1024,2]{0,1:T(2,128)} %param.21) | copy-start | bytes 24580
  81.6 9.9 %copy-start.8 = (bf16[1024,256]{1,0:T(8,128)(2,1)S(1)}, bf16[1024,256]{1,0:T(8,128)(2,1)}, u32[]{:S(2)}) copy-start(bf16[1024,256]{1,0:T(8,128)(2,1)} %param.19) | copy-start | bytes 1572868
  81.6 11.1 %copy-start.3 = (bf16[1024,512]{1,0:T(8,128)(2,1)S(1)}, bf16[1024,512]{1,0:T(8,128)(2,1)}, u32[]{:S(2)}) copy-start(bf16[1024,512]{1,0:T(8,128)(2,1)} %param.20) | copy-start | bytes 3145732
  81.6 175.6 %all-to-all-start = ((bf16[32,2,24,4096]{3,2,1,0:T(8,128)(2,1)}), bf16[32,2,24,4096]{3,2,1,0:T(8,128)(2,1)}, u32[]{:S(2)}, u32[]{:S(2)}) async-start(bf16[32,2,24,4096]{3,2,1,0:T(8,128)(2,1)} %broadcast_select_fusion.2), calls=%async_computation.1 | async-start | bytes 25165824 | tf_op jit(solution)/shard_map/all_to_all | solution.py:175
  90.2 58.4 %all-gather.12.cloned.1.call-start = ((), (), s32[]{:S(2)}) async-start(), calls=%async_computation.6 | async-start | bytes 1351680 | tf_op jit(solution)/shard_map/all_gather | solution.py:29
  105.8 130.8 %all-gather.14.cloned.1.call-start = ((), (), s32[]{:S(2)}) async-start(), calls=%async_computation.7 | async-start | bytes 1351680 | tf_op jit(solution)/shard_map/all_gather | solution.py:29
  148.6 7.9 %copy-start.1 = (f32[4,258,256]{2,1,0:T(8,128)S(1)}, f32[4,258,256]{2,1,0:T(8,128)}, u32[]{:S(2)}) copy-start(f32[4,258,256]{2,1,0:T(8,128)} %all-gather.12.cloned.1.call-done) | copy-start | bytes 3170308
  152.4 233.3 %all-gather.10.cloned.1.call-start = ((), (), s32[]{:S(2)}) async-start(), calls=%async_computation.5 | async-start | bytes 3932160 | tf_op jit(solution)/shard_map/all_gather | solution.py:184
  275.1 1.9 copy-start.4
  275.1 2.0 copy-start.5
  275.1 2.0 copy-start.6
  275.2 2.0 copy-start.7
  275.2 186.9 %reduce-scatter.2.cloned.1.call-start = ((), (), s32[]{:S(2)}) async-start(), calls=%async_computation.4 | async-start | bytes 10485760 | tf_op jit(solution)/shard_map/reduce_scatter | solution.py:127
  283.7 3.2 copy-start.17
  285.7 2.2 copy-start.16
  385.7 3.0 copy-start
  388.7 2.3 copy-start.2
  398.3 4.5 copy-start.11
  398.3 4.8 %copy-start.12 = (f32[512,2]{0,1:T(2,128)S(1)}, f32[512,2]{0,1:T(2,128)}, u32[]{:S(2)}) copy-start(f32[512,2]{0,1:T(2,128)} %param.30) | copy-start | bytes 12292
  398.3 4.8 %copy-start.15 = (f32[512]{0:T(512)S(1)}, f32[512]{0:T(512)}, u32[]{:S(2)}) copy-start(f32[512]{0:T(512)} %param.29) | copy-start | bytes 6148
  398.3 46.2 %all-to-all-start.2 = ((bf16[1024,32,2,24]{0,3,2,1:T(8,128)(2,1)}), bf16[1024,32,2,24]{0,3,2,1:T(8,128)(2,1)S(1)}, u32[]{:S(2)}, u32[]{:S(2)}) async-start(bf16[1024,32,2,24]{0,3,2,1:T(8,128)(2,1)} %copy.168), calls=%async_computation.3 | async-start | bytes 6291456 | tf_op jit(solution)/shard_map/all_to_all | solution.py:193
Sparse Core Ops, SparseCore 0:
  105.9 42.5 all-gather.11
  152.5 84.0 all-gather.13
Sparse Core Ops, SparseCore 1:
  275.3 48.7 all-gather.9
  326.9 99.7 reduce-scatter.1
where the time goes:
time: 477 us; the launch traced here: 470 us
  waiting for transfers between devices  183 us (38%)
  local copies, waits for them, and re-layouts  81.5 us (17%)
  blocking collectives  69.9 us (15%)
  other arithmetic  65.1 us (14%)
  matrix products  39.9 us (8%)
  between operations  16.4 us (3%)
  starting transfers between devices  13.7 us (3%)
    all_gather x2, waiting for transfers between devices, collected_together(): both, at, found = (lax.all_gather(jnp.concatenate(lines), axis), 0, {})  122 us
    all_to_all x1, blocking collectives, expert_half(): lax.all_to_all(down_weight, 'tp', split_axis=2, concat_axis=1, tiled=True)  67.7 us
    all_to_all x1, waiting for transfers between devices, expert_half(): lax.all_to_all(finished, EP, split_axis=1, concat_axis=1, tiled=True)  41.2 us
    gather x1, local copies, waits for them, and re-layouts, expert_half(): normed[slot_token]  24.8 us
    all_to_all x1, waiting for transfers between devices, expert_half(): lax.all_to_all(outgoing, EP, split_axis=0, concat_axis=0, tiled=True)  19.7 us
    another operation x5, other arithmetic  18.2 us
    unnamed x46, local copies, waits for them, and re-layouts  13.6 us
    all_to_all x1, local copies, waits for them, and re-layouts, expert_half(): lax.all_to_all(down_weight, 'tp', split_axis=2, concat_axis=1, tiled=True)  11.3 us
  transfers between devices with their start and end apart: 6, of which 4 were waited for; matrix products, arithmetic and copies ran while one was open for 20% of the time, Pallas kernels for 0%

commit v1 on v0

--- a/solution.py
+++ b/solution.py
@@ -177,7 +177,10 @@
     upward = jnp.einsum("serd,edf->serf", arrived, up_weight, preferred_element_type=jnp.float32)
     hidden = (jax.nn.silu(gate) * upward).astype(jnp.bfloat16)
     unit_width = down_weight.shape[1]
-    own_columns = lax.all_to_all(down_weight, "tp", split_axis=2, concat_axis=1, tiled=True)
+    own_columns = jnp.concatenate(
+        lax.all_to_all(jnp.stack(jnp.split(down_weight, lax.axis_size("tp"), axis=2)), "tp", 0, 0),
+        axis=1,
+    )
     column_count = own_columns.shape[2]
     zero_total = jnp.zeros((column_count, ep_size, local_experts, capacity), jnp.float32)
     total = zero_total

time: 477 us -> 457 us (0.958)
  local copies, waits for them, and re-layouts: 81.5 us -> 69.2 us
  blocking collectives: 69.9 us -> 60.7 us
    all_to_all x1 -> x0, local copies, waits for them, and re-layouts: 11.3 us -> none  [expert_half(): lax.all_to_all(down_weight, 'tp', split_axis=2, concat_axis=1, tiled=True)]
    unnamed x46 -> x43, local copies, waits for them, and re-layouts: 13.6 us -> 3.62 us
    all_to_all x1, blocking collectives: 67.7 us -> 58.5 us  [expert_half(): lax.all_to_all(jnp.stack(jnp.split(down_weight, lax.axis_size('tp'), axis...]
    another operation x5 -> x6, other arithmetic: 18.2 us -> 18.8 us
  transfers between devices with their start and end apart: 6 -> 6, of which waited for: 4 -> 4; matrix products, arithmetic and copies ran while one was open for 20% -> 17% of each run, Pallas kernels for 0% -> 0%
where the time goes in v1:
time: 457 us; the launch traced here: 449 us
  waiting for transfers between devices  183 us (40%)
  local copies, waits for them, and re-layouts  69.2 us (15%)
  other arithmetic  65.9 us (14%)
  blocking collectives  60.7 us (13%)
  matrix products  36.8 us (8%)
  starting transfers between devices  16.6 us (4%)
  between operations  16.5 us (4%)
    all_gather x2, waiting for transfers between devices, collected_together(): both, at, found = (lax.all_gather(jnp.concatenate(lines), axis), 0, {})  122 us
    all_to_all x1, blocking collectives, expert_half(): lax.all_to_all(jnp.stack(jnp.split(down_weight, lax.axis_size('tp'), axis...  58.5 us
    all_to_all x1, waiting for transfers between devices, expert_half(): lax.all_to_all(finished, EP, split_axis=1, concat_axis=1, tiled=True)  41.2 us
    gather x1, local copies, waits for them, and re-layouts, expert_half(): normed[slot_token]  24.8 us
    all_to_all x1, waiting for transfers between devices, expert_half(): lax.all_to_all(outgoing, EP, split_axis=0, concat_axis=0, tiled=True)  19.7 us
    another operation x5, other arithmetic  18.2 us
    select_n x1, other arithmetic, expert_half(): jnp.where(slot_used[:, None], normed[slot_token], jnp.zeros((), jnp.bfloa...  10.6 us
    dot_general x1, matrix products, expert_half(): jnp.einsum('serd,edf->serf', arrived, up_weight, preferred_element_type=j...  10.3 us
  transfers between devices with their start and end apart: 6, of which 4 were waited for; matrix products, arithmetic and copies ran while one was open for 17% of the time, Pallas kernels for 0%

profile of v1, /device:TPU:2, one launch (start us, length us, event | category | flops | bytes accessed | tf_op | source)
XLA Modules:
  0.0 449.4 jit_solution(311819065005290546)
XLA Ops:
  9.4 18.0 %reduce-window.6 = s32[64,8,128]{2,1,0:T(8,128)S(1)} reduce-window(s32[64,8,128]{2,1,0:T(8,128)S(1)} %fusion.71, s32[]{:T(128)} %constant.116.clone.1), window={size=1x1x128 pad=0_0x0_0x127_0}, to_apply=%region_7.8 | reduce-window | flops 8323072 | bytes 524292 | tf_op jit(solution)/shard_map/reduce-window
  28.1 4.3 scatter_custom_fusion.1
  32.4 3.1 fusion.12
  35.5 4.9 %scatter_custom_fusion = pred[1536]{0:T(1024)(128)(4,1)S(1)} fusion(s32[1024]{0:T(1024)S(1)} %bitcast.504, pred[1024]{0:T(1024)(128)(4,1)S(1)} %broadcast.884, pred[]{:T(512)} %constant.134.clone.1), kind=kCustom, calls=%fused_computation.179 | custom fusion | bytes 1537 | tf_op jit(solution)/shard_map/scatter | solution.py:172
  40.5 5.8 %fusion.14 = bf16[512,4096]{1,0:T(8,128)(2,1)} fusion(bf16[512,4096]{1,0:T(8,128)(2,1)} %param.26, f32[4096]{0:T(1024)S(1)} %copy-done.9, f32[512]{0:T(512)S(1)} %add_rsqrt_fusion), kind=kLoop, calls=%fused_computation.29 | loop fusion | flops 8388608 | bytes 8407040 | tf_op jit(solution)/shard_map/convert_element_type | solution.py:158
  46.3 24.8 %gather_fusion = bf16[1536,4096]{1,0:T(8,128)(2,1)} fusion(bf16[512,4096]{1,0:T(8,128)(2,1)} %fusion.14, s32[2048]{0:T(1024)S(1)} %pad_clamp_fusion), kind=kCustom, calls=%fused_computation | custom fusion | bytes 25171968 | tf_op jit(solution)/shard_map/gather | solution.py:173
  71.1 10.6 %broadcast_select_fusion.2 = bf16[32,2,24,4096]{3,2,1,0:T(8,128)(2,1)} fusion(bf16[32,2,24,4096]{3,2,1,0:T(8,128)(2,1)} %bitcast.462, pred[32,2,24]{2,1,0:T(4,128)(4,1)S(1)} %broadcast_in_dim.57), kind=kLoop, calls=%fused_computation.20 | loop fusion | flops 6291456 | bytes 25167360 | tf_op jit(solution)/shard_map/jit(_where)/select_n | solution.py:173
  81.8 8.6 %all-to-all-start.1 = ((bf16[32,2,24,4096]{3,2,1,0:T(8,128)(2,1)}), bf16[32,2,24,4096]{3,2,1,0:T(8,128)(2,1)}, u32[]{:S(2)}, u32[]{:S(2)}) async-start(bf16[32,2,24,4096]{3,2,1,0:T(8,128)(2,1)} %broadcast_select_fusion.2), calls=%async_computation.2 | async-start | bytes 25165824 | tf_op jit(solution)/shard_map/all_to_all | solution.py:175
  94.6 7.8 %while.21 = (s32[]{:T(128)}, f32[2,128,256]{2,1,0:T(8,128)S(1)}, f32[2]{0:T(128)S(1)}, f32[2]{0:T(128)S(1)}, f32[8,2,128,256]{3,2,1,0:T(8,128)}, /*index=5*/f32[...) while((s32[]{:T(128)}, f32[2,128,256]{2,1,0:T(8,128)S(1)}, ...), condition=%wide.region_3.4_spmd.clone, body=%wide.region_2.3_spmd.clone.sunk | while | flops 327699 | bytes 1311534 | solution.py:103
  106.1 42.7 %all-gather.12.cloned.1.call-done = f32[4,258,256]{2,1,0:T(8,128)} async-done(((f32[1,258,256]{2,1,0:T(8,128)}), f32[4,258,256]{2,1,0:T(8,128)}) %all-gather.12.cloned.1.call-update) | async-done | bytes 1056784 | tf_op jit(solution)/shard_map/all_gather | solution.py:29
  157.2 79.7 %all-gather.14.cloned.1.call-done = f32[4,258,256]{2,1,0:T(8,128)} async-done(((f32[1,258,256]{2,1,0:T(8,128)}), f32[4,258,256]{2,1,0:T(8,128)}) %all-gather.14.cloned.1.call-update) | async-done | bytes 1056784 | tf_op jit(solution)/shard_map/all_gather | solution.py:29
  237.7 19.7 %all-to-all-done.1 = bf16[32,2,24,4096]{3,2,1,0:T(8,128)(2,1)} async-done(((bf16[32,2,24,4096]{3,2,1,0:T(8,128)(2,1)}), bf16[32,2,24,4096]{3,2,1,0:T(8,128)(2,1)}, u32[]{:S(2)}, u32[]{:S(2)}) %all-to-all-start.1) | async-done | bytes 12582944 | tf_op jit(solution)/shard_map/all_to_all | solution.py:175
  257.4 7.6 %fusion.10 = f32[2,32,24,256]{3,2,1,0:T(8,128)S(1)} fusion(bf16[32,2,24,4096]{3,2,1,0:T(8,128)(2,1)} %all-to-all-done.1, bf16[2,4096,256]{2,1,0:T(8,128)(2,1)} %param.31), kind=kOutput, calls=%fused_computation.23 | convolution fusion | flops 3221225472 | bytes 18350080 | tf_op jit(solution)/shard_map/serd,edf->serf/dot_general | solution.py:176
  265.1 10.3 %fusion.21 = bf16[32,2,24,256]{3,2,0,1:T(8,128)(2,1)} fusion(f32[2,32,24,256]{3,2,1,0:T(8,128)S(1)} %fusion.10, bf16[2,4096,256]{2,1,0:T(8,128)(2,1)} %param.32, bf16[32,2,24,4096]{3,2,1,0:T(8,128)(2,1)} %all-to-all-done.1), kind=kOutput, calls=%fused_computation.51 | convolution fusion | flops 3223584768 | bytes 19136512 | tf_op jit(solution)/shard_map/serd,edf->serf/dot_general | solution.py:177
  280.3 3.7 fusion.19
  288.3 7.4 %convolution_convert_fusion = bf16[1024,4096]{1,0:T(8,128)(2,1)} fusion(bf16[512,4096]{1,0:T(8,128)(2,1)S(1)} %copy-done.15, f32[64,8,8,128]{3,2,1,0:T(8,128)S(1)} %bitcast.470, f32[512]{0:T(512)S(1)} %copy-done.16), kind=kOutput, calls=%fused_computation.30 | convolution fusion | flops 4300210176 | bytes 14682112 | tf_op jit(solution)/shard_map/dot_general | solution.py:128
  299.0 58.5 %all_to_all.15 = bf16[4,2,256,1024]{3,2,1,0:T(8,128)(2,1)S(1)} all-to-all(bf16[4,2,256,1024]{3,2,1,0:T(8,128)(2,1)S(1)} %pad_maximum_fusion), channel_id=1, replica_groups=mesh['ep_0'=4,'ep_1'=4,'ep_2'=2,'tp'=4] {'tp'}, dimensions={0} | all-to-all | bytes 8388608 | tf_op jit(solution)/shard_map/all_to_all | solution.py:181
  367.7 3.4 add_convert_fusion
  371.1 3.4 copy.182
  374.6 7.5 %all-to-all-start.2 = ((bf16[1024,32,2,24]{0,3,2,1:T(8,128)(2,1)}), bf16[1024,32,2,24]{0,3,2,1:T(8,128)(2,1)S(1)}, u32[]{:S(2)}, u32[]{:S(2)}) async-start(bf16[1024,32,2,24]{0,3,2,1:T(8,128)(2,1)} %copy.182), calls=%async_computation.3 | async-start | bytes 6291456 | tf_op jit(solution)/shard_map/all_to_all | solution.py:196
  382.8 41.2 %all-to-all-done.2 = bf16[1024,32,2,24]{0,3,2,1:T(8,128)(2,1)S(1)} async-done(((bf16[1024,32,2,24]{0,3,2,1:T(8,128)(2,1)}), bf16[1024,32,2,24]{0,3,2,1:T(8,128)(2,1)S(1)}, u32[]{:S(2)}, u32[]{:S(2)}) %all-to-all-start.2) | async-done | bytes 3145760 | tf_op jit(solution)/shard_map/all_to_all | solution.py:196
  424.0 5.4 %gather_fusion.1 = bf16[1024,1024]{1,0:T(8,128)(2,1)} fusion(bf16[1024,1536]{0,1:T(8,128)(2,1)S(1)} %bitcast.461, s32[1024]{0:T(1024)S(1)} %broadcast_clamp_fusion), kind=kCustom, calls=%fused_computation.1 | custom fusion | bytes 4198400 | tf_op jit(solution)/shard_map/jit(_take)/gather | solution.py:198
  429.4 2.8 gather.14
  432.2 9.4 %multiply_reduce_fusion = bf16[1024,512]{0,1:T(8,128)(2,1)} fusion(bf16[1024,512,2]{0,2,1:T(2,128)(2,1)S(1)} %gather.14, pred[512,2]{1,0:T(8,128)(4,1)S(1)} %copy.173, f32[512,2]{1,0:T(8,128)S(1)} %copy.183), kind=kLoop, calls=%fused_computation.35 | loop fusion | flops 3670016 | bytes 3150848 | tf_op jit(solution)/shard_map/reduce_sum | solution.py:200
  (218 shorter events, 49.6 us)
Async XLA Ops:
  9.4 31.1 %copy-start.9 = (f32[4096]{0:T(1024)S(1)}, f32[4096]{0:T(1024)}, u32[]{:S(2)}) copy-start(f32[4096]{0:T(1024)} %param.27) | copy-start | bytes 49156
  81.8 8.7 %copy-start.12 = (f32[1024,2]{0,1:T(2,128)S(1)}, f32[1024,2]{0,1:T(2,128)}, u32[]{:S(2)}) copy-start(f32[1024,2]{0,1:T(2,128)} %param.23) | copy-start | bytes 24580
  81.8 8.7 %copy-start.13 = (f32[1024,2]{0,1:T(2,128)S(1)}, f32[1024,2]{0,1:T(2,128)}, u32[]{:S(2)}) copy-start(f32[1024,2]{0,1:T(2,128)} %param.22) | copy-start | bytes 24580
  81.8 9.5 %copy-start.8 = (f32[1024,2]{0,1:T(2,128)S(1)}, f32[1024,2]{0,1:T(2,128)}, u32[]{:S(2)}) copy-start(f32[1024,2]{0,1:T(2,128)} %param.21) | copy-start | bytes 24580
  81.8 9.9 %copy-start.7 = (bf16[1024,256]{1,0:T(8,128)(2,1)S(1)}, bf16[1024,256]{1,0:T(8,128)(2,1)}, u32[]{:S(2)}) copy-start(bf16[1024,256]{1,0:T(8,128)(2,1)} %param.19) | copy-start | bytes 1572868
  81.8 11.1 %copy-start.2 = (bf16[1024,512]{1,0:T(8,128)(2,1)S(1)}, bf16[1024,512]{1,0:T(8,128)(2,1)}, u32[]{:S(2)}) copy-start(bf16[1024,512]{1,0:T(8,128)(2,1)} %param.20) | copy-start | bytes 3145732
  81.8 175.6 %all-to-all-start.1 = ((bf16[32,2,24,4096]{3,2,1,0:T(8,128)(2,1)}), bf16[32,2,24,4096]{3,2,1,0:T(8,128)(2,1)}, u32[]{:S(2)}, u32[]{:S(2)}) async-start(bf16[32,2,24,4096]{3,2,1,0:T(8,128)(2,1)} %broadcast_select_fusion.2), calls=%async_computation.2 | async-start | bytes 25165824 | tf_op jit(solution)/shard_map/all_to_all | solution.py:175
  90.4 58.4 %all-gather.12.cloned.1.call-start = ((), (), s32[]{:S(2)}) async-start(), calls=%async_computation.6 | async-start | bytes 1351680 | tf_op jit(solution)/shard_map/all_gather | solution.py:29
  106.0 130.8 %all-gather.14.cloned.1.call-start = ((), (), s32[]{:S(2)}) async-start(), calls=%async_computation.7 | async-start | bytes 1351680 | tf_op jit(solution)/shard_map/all_gather | solution.py:29
  148.7 7.5 %copy-start.1 = (f32[4,258,256]{2,1,0:T(8,128)S(1)}, f32[4,258,256]{2,1,0:T(8,128)}, u32[]{:S(2)}) copy-start(f32[4,258,256]{2,1,0:T(8,128)} %all-gather.12.cloned.1.call-done) | copy-start | bytes 3170308
  152.6 207.4 %all-gather.10.cloned.1.call-start = ((), (), s32[]{:S(2)}) async-start(), calls=%async_computation.5 | async-start | bytes 3932160 | tf_op jit(solution)/shard_map/all_gather | solution.py:187
  275.4 2.0 copy-start.3
  275.4 2.0 copy-start.4
  275.4 2.0 copy-start.5
  275.4 2.0 copy-start.6
  275.4 166.2 %reduce-scatter.2.cloned.1.call-start = ((), (), s32[]{:S(2)}) async-start(), calls=%async_computation.4 | async-start | bytes 10485760 | tf_op jit(solution)/shard_map/reduce_scatter | solution.py:127
  284.0 3.2 copy-start.16
  286.0 2.2 copy-start.15
  359.9 3.8 copy-start
  374.6 7.8 %copy-start.10 = (s32[512,2]{0,1:T(2,128)S(1)}, s32[512,2]{0,1:T(2,128)}, u32[]{:S(2)}) copy-start(s32[512,2]{0,1:T(2,128)} %param.28) | copy-start | bytes 12292
  374.6 8.0 %copy-start.11 = (f32[512,2]{0,1:T(2,128)S(1)}, f32[512,2]{0,1:T(2,128)}, u32[]{:S(2)}) copy-start(f32[512,2]{0,1:T(2,128)} %param.30) | copy-start | bytes 12292
  374.6 8.1 %copy-start.14 = (f32[512]{0:T(512)S(1)}, f32[512]{0:T(512)}, u32[]{:S(2)}) copy-start(f32[512]{0:T(512)} %param.29) | copy-start | bytes 6148
  374.6 49.4 %all-to-all-start.2 = ((bf16[1024,32,2,24]{0,3,2,1:T(8,128)(2,1)}), bf16[1024,32,2,24]{0,3,2,1:T(8,128)(2,1)S(1)}, u32[]{:S(2)}, u32[]{:S(2)}) async-start(bf16[1024,32,2,24]{0,3,2,1:T(8,128)(2,1)} %copy.182), calls=%async_computation.3 | async-start | bytes 6291456 | tf_op jit(solution)/shard_map/all_to_all | solution.py:196
Sparse Core Ops, SparseCore 0:
  106.1 42.5 all-gather.11
  152.7 84.1 all-gather.13
Sparse Core Ops, SparseCore 1:
  275.5 65.3 all-gather.9
  343.8 89.0 reduce-scatter.1
